TPU v7x, 32 devices: a whole 2x2x4 slice. The times are simulated.
32 devices in a mesh: fs: 8 (over z, x), tp: 4 (over y, core).
Axes of the slice: x: 2, y: 2, z: 4, core: 2. Of those that a mesh axis runs over, the one named last changes fastest.
Arguments:
- tokens: bfloat16 [4096, 2048], P('fs', 'tp'), may hold values from -6 to 6
- pre_gain: float32 [2048], P('fs'), may hold values from 0.1 to 1.9
- gate_weight: float32 [2048, 6144], P('fs', 'tp'), may hold values from -0.125 to 0.125
- up_weight: float32 [2048, 6144], P('fs', 'tp'), may hold values from -0.125 to 0.125
- down_weight: float32 [2048, 6144], P('fs', 'tp'), may hold values from -0.078125 to 0.078125
- post_gain: float32 [2048], P('tp'), may hold values from 0.1 to 1.9
Outputs:
- result: bfloat16 [4096, 2048], P('fs', 'tp')
- gate_ready: bfloat16 [2048, 6144], P(None, 'tp')
- up_ready: bfloat16 [2048, 6144], P(None, 'tp')
- down_ready: bfloat16 [2048, 6144], P(None, 'tp')
All inputs are finite; a program needn't handle non-finite values.
Results may differ from a plain program's by a relative error of at most 0.015.
Values may be sent and summed in bfloat16 or wider, within the bound.
A program may use at most 128 MiB of HBM per device.

v0:
```python
import jax
import jax.numpy as jnp
from jax import lax
from jax.sharding import PartitionSpec as P

EPS = 1e-06


def shards(tokens, pre_gain, gate_weight, up_weight, down_weight, post_gain):
    gate_local = (pre_gain[:, None] * gate_weight).astype(jnp.bfloat16)
    up_local = (pre_gain[:, None] * up_weight).astype(jnp.bfloat16)
    down_local = down_weight.astype(jnp.bfloat16)
    whole = lax.all_gather(tokens, "tp", axis=1, tiled=True)
    widened = whole.astype(jnp.float32)
    width = whole.shape[1]
    normalized = (
        widened * lax.rsqrt(jnp.mean(widened * widened, axis=1, keepdims=True) + EPS)
    ).astype(jnp.bfloat16)
    contract = (((1,), (1,)), ((), ()))
    gate_full, up_full, down_full = (
        lax.all_gather(gate_local, "fs", axis=0, tiled=True),
        lax.all_gather(up_local, "fs", axis=0, tiled=True),
        lax.all_gather(down_local, "fs", axis=0, tiled=True),
    )
    gate = jnp.dot(normalized, gate_full, preferred_element_type=jnp.float32)
    up = jnp.dot(normalized, up_full, preferred_element_type=jnp.float32)
    hidden = (jax.nn.silu(gate) * up).astype(jnp.bfloat16)
    partial_value = lax.dot_general(hidden, down_full, contract, preferred_element_type=jnp.float32)
    share = lax.psum_scatter(
        partial_value.astype(jnp.bfloat16), "tp", scatter_dimension=1, tiled=True
    ).astype(jnp.float32)
    squares = lax.psum(jnp.sum(share * share, axis=1, keepdims=True), "tp")
    scaling = lax.rsqrt(squares / width + EPS)
    result = (share * scaling * post_gain[None, :]).astype(jnp.bfloat16)
    return (result, gate_full, up_full, down_full)


def solution(mesh):
    return jax.shard_map(
        shards,
        mesh=mesh,
        in_specs=(P("fs", "tp"), P("fs"), P("fs", "tp"), P("fs", "tp"), P("fs", "tp"), P("tp")),
        out_specs=(P("fs", "tp"), P(None, "tp"), P(None, "tp"), P(None, "tp")),
        check_vma=False,
    )
```

profile of v0, /device:TPU:0, one launch (start us, length us, event | category | flops | bytes accessed | tf_op | source)
XLA Modules:
  0.0 406.3 jit_solution(389480162345285521)
XLA Ops:
  7.2 0.0 all-gather.5.cloned.1.call-start
  7.2 0.7 all-gather.5.cloned.1.call-update
  7.9 0.0 copy-start.1
  7.9 0.0 all-gather.7.cloned.1.call-start
  8.0 3.5 multiply_convert_fusion.1
  11.5 0.0 all-gather.7.cloned.1.call-update
  11.5 0.0 all-gather.9.cloned.1.call-start
  11.6 0.7 all-gather.9.cloned.1.call-update
  12.3 0.0 all-gather.11.cloned.1.call-start
  12.3 0.0 copy-done.1
  12.3 1.0 convert_element_type.32
  13.3 0.0 all-gather.11.cloned.1.call-update
  13.3 0.0 reduce-scatter.2.cloned.1.call-start
  13.4 21.5 %all-gather.5.cloned.1.call-done = bf16[512,2048]{1,0:T(8,128)(2,1)} async-done(((bf16[512,512]{1,0:T(8,128)(2,1)}), bf16[512,2048]{1,0:T(8,128)(2,1)}) %all-gather.5.cloned.1.call-update) | async-done | bytes 2097168 | tf_op jit(solution)/shard_map/all_gather | solution.py:13
  34.9 2.1 fusion
  36.9 0.0 copy-start
  37.0 99.4 %all-gather.7.cloned.1.call-done = bf16[2048,1536]{1,0:T(8,128)(2,1)} async-done(((bf16[256,1536]{1,0:T(8,128)(2,1)}), bf16[2048,1536]{1,0:T(8,128)(2,1)}) %all-gather.7.cloned.1.call-update) | async-done | bytes 6291472 | tf_op jit(solution)/shard_map/all_gather | solution.py:21
  136.3 8.5 %fusion.7 = f32[512,1536]{1,0:T(8,128)} fusion(bf16[2048,1536]{1,0:T(8,128)(2,1)} %all-gather.7.cloned.1.call-done, bf16[512,2048]{1,0:T(8,128)(2,1)} %all-gather.5.cloned.1.call-done, f32[512]{0:T(512)S(1)} %add_rsqrt_fusion.1), kind=kOutput, calls=%fused_computation.14 | convolution fusion | flops 3224371200 | bytes 11536384 | tf_op jit(solution)/shard_map/dot_general | solution.py:25
  144.9 0.0 copy-start.2
  144.9 91.1 %all-gather.9.cloned.1.call-done = bf16[2048,1536]{1,0:T(8,128)(2,1)} async-done(((bf16[256,1536]{1,0:T(8,128)(2,1)}), bf16[2048,1536]{1,0:T(8,128)(2,1)}) %all-gather.9.cloned.1.call-update) | async-done | bytes 6291472 | tf_op jit(solution)/shard_map/all_gather | solution.py:22
  236.0 99.5 %all-gather.11.cloned.1.call-done = bf16[2048,1536]{1,0:T(8,128)(2,1)} async-done(((bf16[256,1536]{1,0:T(8,128)(2,1)}), bf16[2048,1536]{1,0:T(8,128)(2,1)}) %all-gather.11.cloned.1.call-update) | async-done | bytes 6291472 | tf_op jit(solution)/shard_map/all_gather | solution.py:23
  335.5 0.0 copy-done
  335.5 13.6 %convolution_convert_fusion = bf16[512,2048]{1,0:T(8,128)(2,1)} fusion(bf16[2048,1536]{1,0:T(8,128)(2,1)} %all-gather.11.cloned.1.call-done, bf16[2048,1536]{1,0:T(8,128)(2,1)} %all-gather.9.cloned.1.call-done, f32[512,1536]{1,0:T(8,128)} %fusion.7, bf16[512,2048]{1,0:T(8,128)(2,1)S(1)} %copy-done, f32[512]{0:T(512)S(1)} %add_rsqrt_fusion.1), kind=kOutput, calls=%fused_computation.6 | convolution fusion | flops 6451363840 | bytes 19924992 | tf_op jit(solution)/shard_map/dot_general | solution.py:28
  349.2 0.0 reduce-scatter.2.cloned.1.call-update
  349.2 29.5 %reduce-scatter.2.cloned.1.call-done = bf16[512,512]{1,0:T(8,128)(2,1)} async-done(((bf16[512,2048]{1,0:T(8,128)(2,1)}), bf16[512,512]{1,0:T(8,128)(2,1)}) %reduce-scatter.2.cloned.1.call-update) | async-done | bytes 524304 | tf_op jit(solution)/shard_map/reduce_scatter | solution.py:29
  378.7 1.2 fusion.3
  379.9 5.8 %psum.7 = f32[512,1]{0,1:T(1,128)S(1)} all-reduce(f32[512,1]{0,1:T(1,128)S(1)} %bitcast.10), channel_id=1, replica_groups=mesh['fs'=8,'tp'=4] {'tp'}, use_global_device_ids=true, to_apply=%region_3.4 | all-reduce | flops 512 | bytes 4096 | tf_op jit(solution)/shard_map/psum | solution.py:32
  385.7 0.0 copy-done.2
  385.7 0.0 slice-start
  385.7 2.2 fusion.5
  387.8 0.0 slice-start.1
  387.8 0.0 slice-start.2
  387.8 6.1 %copy.13 = bf16[2048,1536]{1,0:T(8,128)(2,1)} copy(bf16[2048,1536]{1,0:T(8,128)(2,1)} %all-gather.7.cloned.1.call-done) | data formatting | bytes 12582912
  393.9 0.0 slice-done
  393.9 0.0 slice-done.1
  393.9 0.0 slice-start.3
  393.9 2.8 copy.14
  396.8 0.0 slice-done.2
  396.8 0.3 slice-done.3
  397.0 2.7 copy.15
  (4 shorter events, 0.0 us)
Async XLA Ops:
  7.2 27.7 %all-gather.5.cloned.1.call-start = ((), (), s32[]{:S(2)}) async-start(), calls=%async_computation.1 | async-start | bytes 2621440 | tf_op jit(solution)/shard_map/all_gather | solution.py:13
  7.9 4.4 %copy-start.1 = (f32[256,1536]{1,0:T(8,128)S(1)}, f32[256,1536]{1,0:T(8,128)}, u32[]{:S(2)}) copy-start(f32[256,1536]{1,0:T(8,128)} %param.10) | copy-start | bytes 4718596
  7.9 128.4 %all-gather.7.cloned.1.call-start = ((), (), s32[]{:S(2)}) async-start(), calls=%async_computation.2 | async-start | bytes 7077888 | tf_op jit(solution)/shard_map/all_gather | solution.py:21
  11.5 224.5 %all-gather.9.cloned.1.call-start = ((), (), s32[]{:S(2)}) async-start(), calls=%async_computation.3 | async-start | bytes 7077888 | tf_op jit(solution)/shard_map/all_gather | solution.py:22
  12.3 323.3 %all-gather.11.cloned.1.call-start = ((), (), s32[]{:S(2)}) async-start(), calls=%async_computation.4 | async-start | bytes 7077888 | tf_op jit(solution)/shard_map/all_gather | solution.py:23
  13.3 365.4 %reduce-scatter.2.cloned.1.call-start = ((), (), s32[]{:S(2)}) async-start(), calls=%async_computation.5 | async-start | bytes 2621440 | tf_op jit(solution)/shard_map/reduce_scatter | solution.py:29
  36.9 298.6 %copy-start = (bf16[512,2048]{1,0:T(8,128)(2,1)S(1)}, bf16[512,2048]{1,0:T(8,128)(2,1)}, u32[]{:S(2)}) copy-start(bf16[512,2048]{1,0:T(8,128)(2,1)} %all-gather.5.cloned.1.call-done) | copy-start | bytes 6291460
  144.9 240.8 %copy-start.2 = (f32[512]{0:T(512)S(1)}, f32[512]{0:T(512)}, u32[]{:S(2)}) copy-start(f32[512]{0:T(512)} %param.11) | copy-start | bytes 6148
  385.7 8.2 %slice-start = ((s8[6291456]{0:T(1024)(128)(4,1)}), s8[4194304]{0:T(1024)(128)(4,1)S(1)}, s32[]{:S(2)}) async-start(s8[6291456]{0:T(1024)(128)(4,1)} %bitcast.5), calls=%async_computation.6 | async-start | bytes 8388608
  387.8 6.1 %slice-start.1 = ((s8[6291456]{0:T(1024)(128)(4,1)}), s8[2097152]{0:T(1024)(128)(4,1)S(1)}, s32[]{:S(2)}) async-start(s8[6291456]{0:T(1024)(128)(4,1)} %bitcast.5), calls=%async_computation.7 | async-start | bytes 4194304
  387.8 8.9 %slice-start.2 = ((s8[6291456]{0:T(1024)(128)(4,1)}), s8[4194304]{0:T(1024)(128)(4,1)S(1)}, s32[]{:S(2)}) async-start(s8[6291456]{0:T(1024)(128)(4,1)} %bitcast.7), calls=%async_computation.8 | async-start | bytes 8388608
  393.9 3.1 slice-start.3
Sparse Core Ops, SparseCore 0:
  9.5 25.2 all-gather.4
  37.6 98.6 all-gather.6
  139.1 96.8 all-gather.8
  238.6 96.8 all-gather.10
  349.3 29.3 reduce-scatter.1
where the time goes:
time: 407 us; the launch traced here: 406 us
  waiting for transfers between devices  342 us (84%)
  matrix products  22.2 us (5%)
  between operations  13.8 us (3%)
  local copies, waits for them, and re-layouts  11.9 us (3%)
  other arithmetic  9.99 us (2%)
  blocking collectives  5.76 us (1%)
    all_gather x1, waiting for transfers between devices, shards(): lax.all_gather(down_local, 'fs', axis=0, tiled=True)  99.5 us
    all_gather x1, waiting for transfers between devices, shards(): lax.all_gather(gate_local, 'fs', axis=0, tiled=True)  99.4 us
    all_gather x1, waiting for transfers between devices, shards(): lax.all_gather(up_local, 'fs', axis=0, tiled=True)  91.1 us
    reduce_scatter x1, waiting for transfers between devices, shards(): lax.psum_scatter(partial_value.astype(jnp.bfloat16), 'tp', scatter_dimens...  29.5 us
    all_gather x1, waiting for transfers between devices, shards(): whole = lax.all_gather(tokens, 'tp', axis=1, tiled=True)  21.5 us
    dot_general x1, matrix products, shards(): lax.dot_general(hidden, down_full, contract, preferred_element_type=jnp.f...  13.6 us
    unnamed x17, local copies, waits for them, and re-layouts  11.9 us
    dot_general x1, matrix products, shards(): gate = jnp.dot(normalized, gate_full, preferred_element_type=jnp.float32)  8.54 us
  transfers between devices with their start and end apart: 5, of which 5 were waited for; matrix products, arithmetic and copies ran while one was open for 4% of the time, Pallas kernels for 0%

commit v1 on v0

--- a/solution.py
+++ b/solution.py
@@ -10,7 +10,12 @@
     gate_local = (pre_gain[:, None] * gate_weight).astype(jnp.bfloat16)
     up_local = (pre_gain[:, None] * up_weight).astype(jnp.bfloat16)
     down_local = down_weight.astype(jnp.bfloat16)
-    whole = lax.all_gather(tokens, "tp", axis=1, tiled=True)
+    ring = [tokens]
+    for hop in range(3):
+        ring.append(lax.ppermute(ring[-1], "tp", [(dev, (dev + 1) % 4) for dev in range(4)]))
+    whole = jnp.roll(
+        jnp.concatenate(ring[::-1], axis=1), (lax.axis_index("tp") + 1) * ring[0].shape[1], axis=1
+    )
     widened = whole.astype(jnp.float32)
     width = whole.shape[1]
     normalized = (

time: 407 us -> 383 us (0.941)
  waiting for transfers between devices: 342 us -> 317 us
    all_gather x1, waiting for transfers between devices: 99.4 us -> 70.1 us  [shards(): lax.all_gather(gate_local, 'fs', axis=0, tiled=True)]
    ppermute x0 -> x3, waiting for transfers between devices: none -> 26 us  [shards(): lax.ppermute(ring[-1], 'tp', [(dev, (dev + 1) % 4) for dev in range(4)])]
    all_gather x1 -> x0, waiting for transfers between devices: 21.5 us -> none  [shards(): whole = lax.all_gather(tokens, 'tp', axis=1, tiled=True)]
    unnamed x17 -> x26, local copies, waits for them, and re-layouts: 11.9 us -> 14.3 us
  transfers between devices with their start and end apart: 5 -> 7, of which waited for: 5 -> 7; matrix products, arithmetic and copies ran while one was open for 4% -> 3% of each run, Pallas kernels for 0% -> 0%
where the time goes in v1:
time: 383 us
  waiting for transfers between devices  317 us (83%)
  matrix products  22.7 us (6%)
  local copies, waits for them, and re-layouts  14.4 us (4%)
  between operations  13.9 us (4%)
  other arithmetic  8.44 us (2%)
  blocking collectives  5.76 us (2%)
    all_gather x1, waiting for transfers between devices, shards(): lax.all_gather(down_local, 'fs', axis=0, tiled=True)  99.7 us
    all_gather x1, waiting for transfers between devices, shards(): lax.all_gather(up_local, 'fs', axis=0, tiled=True)  90.5 us
    all_gather x1, waiting for transfers between devices, shards(): lax.all_gather(gate_local, 'fs', axis=0, tiled=True)  70.1 us
    reduce_scatter x1, waiting for transfers between devices, shards(): lax.psum_scatter(partial_value.astype(jnp.bfloat16), 'tp', scatter_dimens...  29.5 us
    ppermute x3, waiting for transfers between devices, shards(): lax.ppermute(ring[-1], 'tp', [(dev, (dev + 1) % 4) for dev in range(4)])  26 us
    unnamed x26, local copies, waits for them, and re-layouts  14.3 us
    dot_general x1, matrix products, shards(): lax.dot_general(hidden, down_full, contract, preferred_element_type=jnp.f...  14.2 us
    dot_general x1, matrix products, shards(): gate = jnp.dot(normalized, gate_full, preferred_element_type=jnp.float32)  8.54 us
  transfers between devices with their start and end apart: 7, of which 7 were waited for; matrix products, arithmetic and copies ran while one was open for 3% of the time, Pallas kernels for 0%

profile of v1, /device:TPU:0, one launch (start us, length us, event | category | flops | bytes accessed | tf_op | source)
XLA Modules:
  0.0 382.5 jit_solution(4125927931957891744)
XLA Ops:
  7.2 0.0 copy-start.2
  7.2 0.0 copy-start
  7.2 0.0 all-gather.4.cloned.1.call-start
  7.2 3.6 multiply_convert_fusion.1
  10.8 0.0 all-gather.4.cloned.1.call-update
  10.8 0.0 all-gather.6.cloned.1.call-start
  10.9 0.7 all-gather.6.cloned.1.call-update
  11.6 0.0 all-gather.8.cloned.1.call-start
  11.6 0.0 copy-done.2
  11.7 1.0 convert_element_type.32
  12.6 0.0 all-gather.8.cloned.1.call-update
  12.6 0.0 reduce-scatter.2.cloned.1.call-start
  12.7 0.0 copy-done
  12.7 0.5 collective-permute-start
  13.2 8.8 %collective-permute-done = bf16[512,512]{1,0:T(8,128)(2,1)S(1)} collective-permute-done((bf16[512,512]{1,0:T(8,128)(2,1)S(1)}, bf16[512,512]{1,0:T(8,128)(2,1)S(1)}, u32[]{:S(2)}, u32[]{:S(2)}) %collective-permute-start) | collective-permute-done | bytes 524320 | tf_op jit(solution)/shard_map/ppermute | solution.py:15
  22.1 0.0 collective-permute-start.1
  22.1 8.6 %collective-permute-done.1 = bf16[512,512]{1,0:T(8,128)(2,1)S(1)} collective-permute-done((bf16[512,512]{1,0:T(8,128)(2,1)S(1)}, bf16[512,512]{1,0:T(8,128)(2,1)S(1)}, u32[]{:S(2)}, u32[]{:S(2)}) %collective-permute-start.1) | collective-permute-done | bytes 524320 | tf_op jit(solution)/shard_map/ppermute | solution.py:15
  30.7 0.0 collective-permute-start.2
  30.7 8.6 %collective-permute-done.2 = bf16[512,512]{1,0:T(8,128)(2,1)S(1)} collective-permute-done((bf16[512,512]{1,0:T(8,128)(2,1)S(1)}, bf16[512,512]{1,0:T(8,128)(2,1)S(1)}, u32[]{:S(2)}, u32[]{:S(2)}) %collective-permute-start.2) | collective-permute-done | bytes 524320 | tf_op jit(solution)/shard_map/ppermute | solution.py:15
  39.3 0.1 constant_dynamic-update-slice_fusion.7
  39.3 0.1 constant_dynamic-update-slice_fusion.6
  39.4 0.1 constant_dynamic-update-slice_fusion.5
  39.5 0.1 constant_dynamic-update-slice_fusion.4
  39.5 0.1 constant_dynamic-update-slice_fusion.3
  39.6 0.1 constant_dynamic-update-slice_fusion.2
  39.7 0.1 constant_dynamic-update-slice_fusion.1
  39.7 0.1 constant_dynamic-update-slice_fusion
  39.8 0.0 copy-start.1
  39.8 2.0 copy-done.1
  41.8 0.5 fusion
  42.3 70.1 %all-gather.4.cloned.1.call-done = bf16[2048,1536]{1,0:T(8,128)(2,1)} async-done(((bf16[256,1536]{1,0:T(8,128)(2,1)}), bf16[2048,1536]{1,0:T(8,128)(2,1)}) %all-gather.4.cloned.1.call-update) | async-done | bytes 6291472 | tf_op jit(solution)/shard_map/all_gather | solution.py:26
  112.4 8.5 %fusion.8 = f32[512,1536]{1,0:T(8,128)} fusion(bf16[2048,1536]{1,0:T(8,128)(2,1)} %all-gather.4.cloned.1.call-done, f32[512]{0:T(512)S(1)} %add_rsqrt_fusion.1, bf16[512,4096]{1,0:T(8,128)(2,1)} %copy-done.1, s32[]{:T(128)S(6)} %select_n.14), kind=kOutput, calls=%fused_computation.14 | convolution fusion | flops 3224371200 | bytes 11536388 | tf_op jit(solution)/shard_map/dot_general | solution.py:30
  121.0 90.5 %all-gather.6.cloned.1.call-done = bf16[2048,1536]{1,0:T(8,128)(2,1)} async-done(((bf16[256,1536]{1,0:T(8,128)(2,1)}), bf16[2048,1536]{1,0:T(8,128)(2,1)}) %all-gather.6.cloned.1.call-update) | async-done | bytes 6291472 | tf_op jit(solution)/shard_map/all_gather | solution.py:27
  211.5 99.7 %all-gather.8.cloned.1.call-done = bf16[2048,1536]{1,0:T(8,128)(2,1)} async-done(((bf16[256,1536]{1,0:T(8,128)(2,1)}), bf16[2048,1536]{1,0:T(8,128)(2,1)}) %all-gather.8.cloned.1.call-update) | async-done | bytes 6291472 | tf_op jit(solution)/shard_map/all_gather | solution.py:28
  311.2 14.2 %convolution_convert_fusion = bf16[512,2048]{1,0:T(8,128)(2,1)} fusion(bf16[2048,1536]{1,0:T(8,128)(2,1)} %all-gather.8.cloned.1.call-done, bf16[2048,1536]{1,0:T(8,128)(2,1)} %all-gather.6.cloned.1.call-done, f32[512,1536]{1,0:T(8,128)} %fusion.8, f32[512]{0:T(512)S(1)} %add_rsqrt_fusion.1, bf16[512,4096]{1,0:T(8,128)(2,1)} %copy-done.1, s32[]{:T(128)S(6)} %select_n.14), kind=kOutput, calls=%fused_computation.6 | convolution fusion | flops 6451363840 | bytes 19924996 | tf_op jit(solution)/shard_map/dot_general | solution.py:33
  325.4 0.0 reduce-scatter.2.cloned.1.call-update
  325.4 29.5 %reduce-scatter.2.cloned.1.call-done = bf16[512,512]{1,0:T(8,128)(2,1)} async-done(((bf16[512,2048]{1,0:T(8,128)(2,1)}), bf16[512,512]{1,0:T(8,128)(2,1)}) %reduce-scatter.2.cloned.1.call-update) | async-done | bytes 524304 | tf_op jit(solution)/shard_map/reduce_scatter | solution.py:34
  354.9 1.2 fusion.3
  356.1 5.8 %psum.7 = f32[512,1]{0,1:T(1,128)S(1)} all-reduce(f32[512,1]{0,1:T(1,128)S(1)} %bitcast.10), channel_id=1, replica_groups=mesh['fs'=8,'tp'=4] {'tp'}, use_global_device_ids=true, to_apply=%region_3.4 | all-reduce | flops 512 | bytes 4096 | tf_op jit(solution)/shard_map/psum | solution.py:37
  361.9 0.0 copy-done.3
  361.9 0.0 slice-start
  361.9 2.2 fusion.5
  364.1 6.1 %copy.20 = bf16[2048,1536]{1,0:T(8,128)(2,1)} copy(bf16[2048,1536]{1,0:T(8,128)(2,1)} %all-gather.4.cloned.1.call-done) | data formatting | bytes 12582912
  370.2 0.0 slice-done
  370.2 0.0 slice-done.1
  370.2 2.8 copy.21
  373.0 0.3 slice-done.3
  373.3 2.7 copy.22
  (9 shorter events, 0.0 us)
Async XLA Ops:
  7.2 4.5 %copy-start.2 = (f32[256,1536]{1,0:T(8,128)S(1)}, f32[256,1536]{1,0:T(8,128)}, u32[]{:S(2)}) copy-start(f32[256,1536]{1,0:T(8,128)} %param.10) | copy-start | bytes 4718596
  7.2 5.5 %copy-start = (bf16[512,512]{1,0:T(8,128)(2,1)S(1)}, bf16[512,512]{1,0:T(8,128)(2,1)}, u32[]{:S(2)}) copy-start(bf16[512,512]{1,0:T(8,128)(2,1)} %param.6) | copy-start | bytes 1572868
  7.2 105.2 %all-gather.4.cloned.1.call-start = ((), (), s32[]{:S(2)}) async-start(), calls=%async_computation.1 | async-start | bytes 7077888 | tf_op jit(solution)/shard_map/all_gather | solution.py:26
  10.8 200.7 %all-gather.6.cloned.1.call-start = ((), (), s32[]{:S(2)}) async-start(), calls=%async_computation.2 | async-start | bytes 7077888 | tf_op jit(solution)/shard_map/all_gather | solution.py:27
  11.6 299.6 %all-gather.8.cloned.1.call-start = ((), (), s32[]{:S(2)}) async-start(), calls=%async_computation.3 | async-start | bytes 7077888 | tf_op jit(solution)/shard_map/all_gather | solution.py:28
  12.6 342.3 %reduce-scatter.2.cloned.1.call-start = ((), (), s32[]{:S(2)}) async-start(), calls=%async_computation.4 | async-start | bytes 2621440 | tf_op jit(solution)/shard_map/reduce_scatter | solution.py:34
  12.7 9.4 %collective-permute-start = (bf16[512,512]{1,0:T(8,128)(2,1)S(1)}, bf16[512,512]{1,0:T(8,128)(2,1)S(1)}, u32[]{:S(2)}, u32[]{:S(2)}) collective-permute-start(bf16[512,512]{1,0:T(8,128)(2,1)S(1)} %copy-done), channel_id=1, source_target_pairs={{0,1},{1,2},{2,3},{3,0},{4,5},{5,6},{6,7},{7,4},{8,9},{9,10},{10,1... | collective-permute-start | bytes 1572872 | tf_op jit(solution)/shard_map/ppermute | solution.py:15
  22.1 8.6 %collective-permute-start.1 = (bf16[512,512]{1,0:T(8,128)(2,1)S(1)}, bf16[512,512]{1,0:T(8,128)(2,1)S(1)}, u32[]{:S(2)}, u32[]{:S(2)}) collective-permute-start(bf16[512,512]{1,0:T(8,128)(2,1)S(1)} %collective-permute-done), channel_id=1, source_target_pairs={{0,1},{1,2},{2,3},{3,0},{4,5},{5,6},{6,7},{7,4},{8,9},{9,10},{10,1... | collective-permute-start | bytes 1572872 | tf_op jit(solution)/shard_map/ppermute | solution.py:15
  30.7 8.6 %collective-permute-start.2 = (bf16[512,512]{1,0:T(8,128)(2,1)S(1)}, bf16[512,512]{1,0:T(8,128)(2,1)S(1)}, u32[]{:S(2)}, u32[]{:S(2)}) collective-permute-start(bf16[512,512]{1,0:T(8,128)(2,1)S(1)} %collective-permute-done.1), channel_id=1, source_target_pairs={{0,1},{1,2},{2,3},{3,0},{4,5},{5,6},{6,7},{7,4},{8,9},{9,10},{10,1... | collective-permute-start | bytes 1572872 | tf_op jit(solution)/shard_map/ppermute | solution.py:15
  39.8 2.0 copy-start.1
  120.9 241.0 %copy-start.3 = (f32[512]{0:T(512)S(1)}, f32[512]{0:T(512)}, u32[]{:S(2)}) copy-start(f32[512]{0:T(512)} %param.11) | copy-start | bytes 6148
  361.9 8.2 %slice-start = ((s8[6291456]{0:T(1024)(128)(4,1)}), s8[4194304]{0:T(1024)(128)(4,1)S(1)}, s32[]{:S(2)}) async-start(s8[6291456]{0:T(1024)(128)(4,1)} %bitcast.5), calls=%async_computation.5 | async-start | bytes 8388608
  364.1 6.1 %slice-start.1 = ((s8[6291456]{0:T(1024)(128)(4,1)}), s8[2097152]{0:T(1024)(128)(4,1)S(1)}, s32[]{:S(2)}) async-start(s8[6291456]{0:T(1024)(128)(4,1)} %bitcast.5), calls=%async_computation.6 | async-start | bytes 4194304
  364.1 8.9 %slice-start.2 = ((s8[6291456]{0:T(1024)(128)(4,1)}), s8[4194304]{0:T(1024)(128)(4,1)S(1)}, s32[]{:S(2)}) async-start(s8[6291456]{0:T(1024)(128)(4,1)} %bitcast.7), calls=%async_computation.7 | async-start | bytes 8388608
  370.2 3.1 slice-start.3
Sparse Core Ops, SparseCore 0:
  11.0 101.3 all-gather.3
  114.6 96.8 all-gather.5
  214.3 96.8 all-gather.7
  325.5 29.3 reduce-scatter.1
